TPU v7x, 32 devices: a whole 2x2x4 slice. The times are simulated.
32 devices in a mesh: sp: 16 (over z, y, x), tp: 2 (over core).
Axes of the slice: x: 2, y: 2, z: 4, core: 2. Of those that a mesh axis runs over, the one named last changes fastest.
Arguments:
- queries: bfloat16 [4096, 1024], P('sp', 'tp'), may hold values from -12 to 12
- keys: bfloat16 [4096, 1024], P('sp', 'tp'), may hold values from -6 to 6
- values: bfloat16 [4096, 1024], P('sp', 'tp'), may hold values from -6 to 6
- w_out: bfloat16 [1024, 2048], P(None, 'tp'), may hold values from -0.375 to 0.375
Outputs:
- mixed: bfloat16 [4096, 2048], P('sp', 'tp')
All inputs are finite; a program needn't handle non-finite values.
Results may differ from a plain program's by a relative error of at most 0.0056.
Values may be sent and summed in bfloat16 or wider, within the bound.
A program may use at most 64 MiB of HBM per device.

v0:
```python
import jax
import jax.numpy as jnp
from jax import lax
from jax.sharding import PartitionSpec as P

HEAD_DIM = 128
SIDE_KEY_COUNT = 64
MIDDLE_DILATION = 4
FAR_DILATION = 16


def from_behind(value, axis, steps):
    count = lax.axis_size(axis)
    first, last = (max(0, -steps), min(count, count - steps))
    return lax.ppermute(value, axis, [(source, source + steps) for source in range(first, last)])


def band_scores(queries, window_keys, start_position, sequence_length, dilation_step):
    nearby_rows, columns = queries.shape
    heads = columns // HEAD_DIM
    residue_rows = nearby_rows // dilation_step
    blocks = residue_rows // residue_rows
    span = residue_rows + 2 * SIDE_KEY_COUNT
    laid = jnp.transpose(
        window_keys.reshape(2, residue_rows + 2 * SIDE_KEY_COUNT, dilation_step, heads, HEAD_DIM),
        (0, 2, 3, 1, 4),
    )
    grouped = jnp.transpose(
        queries.reshape(blocks, residue_rows, dilation_step, heads, HEAD_DIM), (0, 2, 3, 1, 4)
    )
    query_idx = jnp.arange(residue_rows, dtype=jnp.int32)[:, None]
    key_idx = jnp.arange(span, dtype=jnp.int32)[None, :]
    in_band = (key_idx >= query_idx) & (key_idx <= query_idx + 2 * SIDE_KEY_COUNT)
    residues = jnp.arange(dilation_step, dtype=jnp.int32)[:, None, None, None]
    scale = HEAD_DIM ** (-0.5)

    def one_block(inputs):
        number, query_block = inputs
        first_row = number * residue_rows
        scores = (
            jnp.einsum("rhqe,rhke->rhqk", query_block, laid[0], preferred_element_type=jnp.float32)
            * scale
        )
        key_pos = (
            start_position
            + (first_row + key_idx[None, None] - SIDE_KEY_COUNT) * dilation_step
            + residues
        )
        allowed = in_band[None, None] & (key_pos >= 0) & (key_pos < sequence_length)
        scores = jnp.where(allowed, scores, -jnp.inf)
        maximum = jnp.max(scores, axis=-1, keepdims=True)
        raised = jnp.exp(scores - maximum)
        denominator = jnp.sum(raised, axis=-1, keepdims=True)
        weights = (raised / denominator).astype(jnp.bfloat16)
        attended = jnp.einsum(
            "rhqk,rhke->rhqe", weights, laid[1], preferred_element_type=jnp.float32
        )
        log_den = (maximum + jnp.log(denominator))[..., 0]
        return (attended, log_den)

    outputs, log_dens = lax.map(one_block, (jnp.arange(blocks, dtype=jnp.int32), grouped))
    attended = jnp.transpose(outputs, (0, 3, 1, 2, 4)).reshape(nearby_rows, heads, HEAD_DIM)
    log_den = jnp.transpose(log_dens, (0, 3, 1, 2)).reshape(nearby_rows, heads)
    return (attended, log_den)


def far_blocks(stacked_groups, hop_count):
    offsets = list(range(hop_count, 0, -1)) + list(range(-1, -hop_count - 1, -1))
    moved = [from_behind(stacked_groups, "sp", offset) for offset in offsets]
    return moved[:hop_count] + [stacked_groups] + moved[hop_count:]


def per_device(queries, keys, values, w_out):
    nearby_rows, columns = queries.shape
    sequence_length = nearby_rows * lax.axis_size("sp")
    start_position = lax.axis_index("sp") * nearby_rows
    stacked_groups = jnp.stack([keys, values])
    hop_count = -(-(SIDE_KEY_COUNT * FAR_DILATION) // nearby_rows)
    extended = jnp.concatenate(far_blocks(stacked_groups, hop_count), axis=1)

    def window_keys(dilation_step):
        padding = SIDE_KEY_COUNT * dilation_step
        return lax.slice_in_dim(
            extended,
            hop_count * nearby_rows - padding,
            (hop_count + 1) * nearby_rows + padding,
            axis=1,
        )

    nearby = window_keys(1)
    middle_group = window_keys(MIDDLE_DILATION)
    distant_group = window_keys(FAR_DILATION)
    group_results = [
        band_scores(queries, nearby, start_position, sequence_length, 1),
        band_scores(queries, middle_group, start_position, sequence_length, MIDDLE_DILATION),
        band_scores(queries, distant_group, start_position, sequence_length, FAR_DILATION),
    ]
    stacked_out = jnp.stack([item[0] for item in group_results])
    stacked_den = jnp.stack([item[1] for item in group_results])
    shares = jax.nn.softmax(stacked_den, axis=0)
    attended = (
        jnp.sum(shares[..., None] * stacked_out, axis=0)
        .astype(jnp.bfloat16)
        .reshape(nearby_rows, columns)
    )
    mixed = jnp.dot(
        lax.all_gather(attended, "tp", axis=1, tiled=True),
        w_out,
        preferred_element_type=jnp.float32,
    )
    return mixed.astype(jnp.bfloat16)


def solution(mesh):
    in_specs = (P("sp", "tp"), P("sp", "tp"), P("sp", "tp"), P(None, "tp"))
    out_specs = P("sp", "tp")
    return jax.shard_map(
        per_device, mesh=mesh, in_specs=in_specs, out_specs=out_specs, check_vma=False
    )
```

profile of v0, /device:TPU:17, one launch (start us, length us, event | category | flops | bytes accessed | tf_op | source)
XLA Modules:
  0.0 139.6 jit_solution(15422659111726366971)
XLA Ops:
  0.0 1.2 copy.49
  1.2 1.1 copy.50
  2.3 0.8 pad_maximum_fusion.1
  3.2 3.2 %collective-permute-start.2 = (bf16[2,256,512]{1,2,0:T(8,128)(2,1)}, bf16[2,256,512]{1,2,0:T(8,128)(2,1)}, u32[]{:S(2)}, u32[]{:S(2)}) collective-permute-start(bf16[2,256,512]{1,2,0:T(8,128)(2,1)} %pad_maximum_fusion.1), channel_id=1, source_target_pairs={{0,8},{2,10},{4,12},{6,14},{8,16},{10,18},{12,20},{14,22},{16,24},... | collective-permute-start | bytes 1572872 | tf_op jit(solution)/shard_map/ppermute | solution.py:15
  6.4 4.1 %collective-permute-start.3 = (bf16[2,256,512]{1,2,0:T(8,128)(2,1)}, bf16[2,256,512]{1,2,0:T(8,128)(2,1)}, u32[]{:S(2)}, u32[]{:S(2)}) collective-permute-start(bf16[2,256,512]{1,2,0:T(8,128)(2,1)} %pad_maximum_fusion.1), channel_id=1, source_target_pairs={{0,6},{2,8},{4,10},{6,12},{8,14},{10,16},{12,18},{14,20},{16,22},{... | collective-permute-start | bytes 1572872 | tf_op jit(solution)/shard_map/ppermute | solution.py:15
  10.5 1.9 %collective-permute-start.4 = (bf16[2,256,512]{1,2,0:T(8,128)(2,1)}, bf16[2,256,512]{1,2,0:T(8,128)(2,1)}, u32[]{:S(2)}, u32[]{:S(2)}) collective-permute-start(bf16[2,256,512]{1,2,0:T(8,128)(2,1)} %pad_maximum_fusion.1), channel_id=1, source_target_pairs={{0,4},{2,6},{4,8},{6,10},{8,12},{10,14},{12,16},{14,18},{16,20},{1... | collective-permute-start | bytes 1572872 | tf_op jit(solution)/shard_map/ppermute | solution.py:15
  12.4 2.2 %collective-permute-start = (bf16[2,256,512]{1,2,0:T(8,128)(2,1)}, bf16[2,256,512]{1,2,0:T(8,128)(2,1)}, u32[]{:S(2)}, u32[]{:S(2)}) collective-permute-start(bf16[2,256,512]{1,2,0:T(8,128)(2,1)} %pad_maximum_fusion.1), channel_id=1, source_target_pairs={{0,2},{2,4},{4,6},{6,8},{8,10},{10,12},{12,14},{14,16},{16,18},{18... | collective-permute-start | bytes 1572872 | tf_op jit(solution)/shard_map/ppermute | solution.py:15
  14.6 4.9 %collective-permute-start.1 = (bf16[2,256,512]{1,2,0:T(8,128)(2,1)}, bf16[2,256,512]{1,2,0:T(8,128)(2,1)S(1)}, u32[]{:S(2)}, u32[]{:S(2)}) collective-permute-start(bf16[2,256,512]{1,2,0:T(8,128)(2,1)} %pad_maximum_fusion.1), channel_id=1, source_target_pairs={{2,0},{4,2},{6,4},{8,6},{10,8},{12,10},{14,12},{16,14},{18,16},{20... | collective-permute-start | bytes 1572872 | tf_op jit(solution)/shard_map/ppermute | solution.py:15
  19.7 0.7 and_and_fusion.1
  20.3 0.8 fusion.18
  21.2 0.8 reshape.466
  22.0 0.8 reshape.464
  22.8 0.8 reshape.461
  23.6 3.4 %collective-permute-start.5 = (bf16[2,256,512]{1,2,0:T(8,128)(2,1)}, bf16[2,256,512]{1,2,0:T(8,128)(2,1)}, u32[]{:S(2)}, u32[]{:S(2)}) collective-permute-start(bf16[2,256,512]{1,2,0:T(8,128)(2,1)} %pad_maximum_fusion.1), channel_id=1, source_target_pairs={{4,0},{6,2},{8,4},{10,6},{12,8},{14,10},{16,12},{18,14},{20,16},{2... | collective-permute-start | bytes 1572872 | tf_op jit(solution)/shard_map/ppermute | solution.py:15
  27.0 1.9 %constant_dynamic-update-slice_fusion.8 = bf16[2,2304,512]{1,2,0:T(8,128)(2,1)} fusion(bf16[2,256,512]{1,2,0:T(8,128)(2,1)} %collective-permute-done.2), kind=kLoop, calls=%fused_computation.63 | loop fusion | bytes 1048576
  28.9 27.7 %collective-permute-done = bf16[2,256,512]{1,2,0:T(8,128)(2,1)} collective-permute-done((bf16[2,256,512]{1,2,0:T(8,128)(2,1)}, bf16[2,256,512]{1,2,0:T(8,128)(2,1)}, u32[]{:S(2)}, u32[]{:S(2)}) %collective-permute-start) | collective-permute-done | bytes 524320 | tf_op jit(solution)/shard_map/ppermute | solution.py:15
  56.6 1.9 %collective-permute-start.6 = (bf16[2,256,512]{1,2,0:T(8,128)(2,1)}, bf16[2,256,512]{1,2,0:T(8,128)(2,1)}, u32[]{:S(2)}, u32[]{:S(2)}) collective-permute-start(bf16[2,256,512]{1,2,0:T(8,128)(2,1)} %pad_maximum_fusion.1), channel_id=1, source_target_pairs={{6,0},{8,2},{10,4},{12,6},{14,8},{16,10},{18,12},{20,14},{22,16},{... | collective-permute-start | bytes 1572872 | tf_op jit(solution)/shard_map/ppermute | solution.py:15
  58.6 7.2 %collective-permute-done.1 = bf16[2,256,512]{1,2,0:T(8,128)(2,1)S(1)} collective-permute-done((bf16[2,256,512]{1,2,0:T(8,128)(2,1)}, bf16[2,256,512]{1,2,0:T(8,128)(2,1)S(1)}, u32[]{:S(2)}, u32[]{:S(2)}) %collective-permute-start.1) | collective-permute-done | bytes 524320 | tf_op jit(solution)/shard_map/ppermute | solution.py:15
  65.8 5.1 %collective-permute-start.7 = (bf16[2,256,512]{1,2,0:T(8,128)(2,1)}, bf16[2,256,512]{1,2,0:T(8,128)(2,1)}, u32[]{:S(2)}, u32[]{:S(2)}) collective-permute-start(bf16[2,256,512]{1,2,0:T(8,128)(2,1)} %pad_maximum_fusion.1), channel_id=1, source_target_pairs={{8,0},{10,2},{12,4},{14,6},{16,8},{18,10},{20,12},{22,14},{24,16},... | collective-permute-start | bytes 1572872 | tf_op jit(solution)/shard_map/ppermute | solution.py:15
  70.8 2.3 %pad_maximum_fusion = bf16[2,768,512]{1,2,0:T(8,128)(2,1)} fusion(bf16[2,256,512]{1,2,0:T(8,128)(2,1)S(1)} %collective-permute-done.1, bf16[1,256,512]{1,2,0:T(8,128)(2,1)S(1)} %bitcast.133, bf16[1,256,512]{1,2,0:T(8,128)(2,1)S(1)} %bitcast.130, bf16[2,256,512]{1,2,0:T(8,128)(2,1)} %collective-permute-done), kind=kLoop, calls=%fused_computation.5 | loop fusion | flops 6291456 | bytes 3145728 | tf_op jit(solution)/shard_map/concatenate | solution.py:79
  73.2 1.9 %constant_dynamic-update-slice_fusion.7 = bf16[2,2304,512]{1,2,0:T(8,128)(2,1)} fusion(bf16[2,2304,512]{1,2,0:T(8,128)(2,1)} %constant_dynamic-update-slice_fusion.8, bf16[2,256,512]{1,2,0:T(8,128)(2,1)} %collective-permute-done.3), kind=kLoop, calls=%fused_computation.62 | loop fusion | bytes 1048576
  75.1 1.9 %constant_dynamic-update-slice_fusion.6 = bf16[2,2304,512]{1,2,0:T(8,128)(2,1)} fusion(bf16[2,2304,512]{1,2,0:T(8,128)(2,1)} %constant_dynamic-update-slice_fusion.7, bf16[2,256,512]{1,2,0:T(8,128)(2,1)} %collective-permute-done.4), kind=kLoop, calls=%fused_computation.61 | loop fusion | bytes 1048576
  77.0 1.9 %constant_dynamic-update-slice_fusion.5 = bf16[2,2304,512]{1,2,0:T(8,128)(2,1)} fusion(bf16[2,2304,512]{1,2,0:T(8,128)(2,1)} %constant_dynamic-update-slice_fusion.6, bf16[2,256,512]{1,2,0:T(8,128)(2,1)} %collective-permute-done), kind=kLoop, calls=%fused_computation.60 | loop fusion | bytes 1048576
  78.9 2.6 %copy.53 = bf16[2,768,512]{2,1,0:T(8,128)(2,1)} copy(bf16[2,768,512]{1,2,0:T(8,128)(2,1)} %pad_maximum_fusion) | data formatting | bytes 3145728 | tf_op jit(solution)/shard_map/concatenate | solution.py:79
  81.6 1.6 %slice.37 = bf16[2,384,512]{1,2,0:T(8,128)(2,1)S(1)} slice(bf16[2,768,512]{1,2,0:T(8,128)(2,1)} %pad_maximum_fusion), slice={[0:2], [192:576], [0:512]} | slice | bytes 1572864 | tf_op jit(solution)/shard_map/slice | solution.py:83
  83.2 0.9 constant_dynamic-update-slice_fusion.4
  84.0 0.9 constant_dynamic-update-slice_fusion.3
  84.9 1.9 %constant_dynamic-update-slice_fusion.2 = bf16[2,2304,512]{1,2,0:T(8,128)(2,1)} fusion(bf16[2,2304,512]{1,2,0:T(8,128)(2,1)} %constant_dynamic-update-slice_fusion.3, bf16[2,256,512]{1,2,0:T(8,128)(2,1)} %collective-permute-done.5), kind=kLoop, calls=%fused_computation.57 | loop fusion | bytes 1048576
  86.8 1.9 %constant_dynamic-update-slice_fusion.1 = bf16[2,2304,512]{1,2,0:T(8,128)(2,1)} fusion(bf16[2,2304,512]{1,2,0:T(8,128)(2,1)} %constant_dynamic-update-slice_fusion.2, bf16[2,256,512]{1,2,0:T(8,128)(2,1)} %collective-permute-done.6), kind=kLoop, calls=%fused_computation.56 | loop fusion | bytes 1048576
  88.7 1.9 %constant_dynamic-update-slice_fusion = bf16[2,2304,512]{1,2,0:T(8,128)(2,1)} fusion(bf16[2,2304,512]{1,2,0:T(8,128)(2,1)} %constant_dynamic-update-slice_fusion.1, bf16[2,256,512]{1,2,0:T(8,128)(2,1)} %collective-permute-done.7), kind=kLoop, calls=%fused_computation.55 | loop fusion | bytes 1048576 | tf_op jit(solution)/shard_map/concatenate | solution.py:79
  90.6 6.7 %copy.57 = bf16[2,2304,512]{2,1,0:T(8,128)(2,1)} copy(bf16[2,2304,512]{1,2,0:T(8,128)(2,1)} %constant_dynamic-update-slice_fusion) | data formatting | bytes 9437184 | tf_op jit(solution)/shard_map/concatenate | solution.py:79
  97.3 7.7 %reshape.465 = bf16[2,144,16,4,128]{4,3,2,1,0:T(4,128)(2,1)} reshape(bf16[2,2304,512]{2,1,0:T(8,128)(2,1)} %copy.57) | data formatting | bytes 9437184 | tf_op jit(solution)/shard_map/reshape | solution.py:25
  105.0 7.8 %copy.88 = bf16[2,144,16,4,128]{4,1,3,2,0:T(8,128)(2,1)S(1)} copy(bf16[2,144,16,4,128]{4,3,2,1,0:T(4,128)(2,1)} %reshape.465) | data formatting | bytes 9437184 | tf_op jit(solution)/shard_map/reshape | solution.py:25
  112.9 1.4 %fusion.37 = (f32[16,4,16]{2,1,0:T(4,128)S(1)}, f32[16,4,16,144]{3,2,1,0:T(8,128)S(1)}) fusion(bf16[1,16,16,4,128]{4,3,2,1,0:T(4,128)(2,1)S(1)} %copy-done.13, bf16[2,16,4,144,128]{4,3,2,1,0:T(8,128)(2,1)S(1)} %bitcast.127, pred[16,16,144]{2,1,0:T(8,128)(4,1)S(1)} %and_and_fusion), kind=kOutput, calls=%fused_computation.90 | convolution fusion | flops 38190080 | bytes 3280896 | tf_op jit(solution)/shard_map/while/body/eval_jaxpr/rhqe,rhke->rhqk/dot_general | solution.py:41
  114.3 0.7 copy-done.1
  115.1 1.0 copy-done.7
  116.8 3.5 %reshape.463 = bf16[2,192,4,4,128]{4,3,2,1,0:T(4,128)(2,1)} reshape(bf16[2,768,512]{2,1,0:T(8,128)(2,1)} %copy.53) | data formatting | bytes 3145728 | tf_op jit(solution)/shard_map/reshape | solution.py:25
  120.3 1.9 %copy.89 = bf16[2,192,4,4,128]{4,1,3,2,0:T(8,128)(2,1)S(1)} copy(bf16[2,192,4,4,128]{4,3,2,1,0:T(4,128)(2,1)} %reshape.463) | data formatting | bytes 3145728 | tf_op jit(solution)/shard_map/reshape | solution.py:25
  122.1 1.2 copy-done.5
  123.3 0.7 fusion.38
  124.5 0.6 copy-done.8
  125.5 2.9 %fusion.9 = f32[1,16,16,4,128]{4,1,3,2,0:T(8,128)S(1)} fusion(bf16[2,16,4,144,128]{4,3,2,1,0:T(8,128)(2,1)} %bitcast.128, f32[16,4,16,144]{3,2,1,0:T(8,128)} %copy-done.7, f32[16,4,16]{2,1,0:T(4,128)S(1)} %fusion.11, f32[16,4,16]{2,1,0:T(4,128)S(1)} %get-tuple-element.58), kind=kOutput, calls=%fused_computation.22 | convolution fusion | flops 38191104 | bytes 3940352 | tf_op jit(solution)/shard_map/while/body/eval_jaxpr/rhqk,rhke->rhqe/dot_general | solution.py:55
  128.5 1.3 convolution_bitcast_fusion
  129.7 1.2 copy.51
  130.9 1.5 %fusion.39 = (f32[4,256]{1,0:T(4,128)S(1)}, f32[4,256,384]{1,2,0:T(8,128)S(1)}) fusion(bf16[1,256,1,4,128]{4,3,1,2,0:T(4,128)(2,1)} %reshape.461, bf16[2,1,4,384,128]{4,3,2,1,0:T(8,128)(2,1)} %bitcast.141, pred[256,384]{0,1:T(8,128)(4,1)S(1)} %copy-done.14), kind=kOutput, calls=%fused_computation.92 | convolution fusion | flops 101841920 | bytes 2330624 | tf_op jit(solution)/shard_map/while/body/eval_jaxpr/rhqe,rhke->rhqk/dot_general | solution.py:41
  132.7 0.5 convolution_bitcast_fusion.1
  134.7 3.4 %all_gather.3 = bf16[256,1024]{0,1:T(8,128)(2,1)S(1)} all-gather(bf16[256,512]{0,1:T(8,128)(2,1)S(1)} %bitcast.140), channel_id=1, replica_groups=mesh['sp'=16,'tp'=2] {'tp'}, dimensions={1}, use_global_device_ids=true | all-gather | bytes 786432 | tf_op jit(solution)/shard_map/all_gather | solution.py:107
  138.1 1.5 %convolution_convert_fusion = bf16[256,1024]{1,0:T(8,128)(2,1)} fusion(bf16[256,1024]{0,1:T(8,128)(2,1)S(1)} %all_gather.3, bf16[1024,1024]{1,0:T(8,128)(2,1)S(1)} %copy-done), kind=kOutput, calls=%fused_computation.19 | convolution fusion | flops 537133056 | bytes 3145728 | tf_op jit(solution)/shard_map/dot_general | solution.py:106
  (63 shorter events, 3.5 us)
Async XLA Ops:
  0.0 138.1 %copy-start = (bf16[1024,1024]{1,0:T(8,128)(2,1)S(1)}, bf16[1024,1024]{1,0:T(8,128)(2,1)}, u32[]{:S(2)}) copy-start(bf16[1024,1024]{1,0:T(8,128)(2,1)} %param.7) | copy-start | bytes 6291460
  0.0 21.2 %copy-start.2 = (bf16[256,512]{1,0:T(8,128)(2,1)S(1)}, bf16[256,512]{1,0:T(8,128)(2,1)}, u32[]{:S(2)}) copy-start(bf16[256,512]{1,0:T(8,128)(2,1)} %param.4) | copy-start | bytes 786436
  3.2 20.4 %collective-permute-start.2 = (bf16[2,256,512]{1,2,0:T(8,128)(2,1)}, bf16[2,256,512]{1,2,0:T(8,128)(2,1)}, u32[]{:S(2)}, u32[]{:S(2)}) collective-permute-start(bf16[2,256,512]{1,2,0:T(8,128)(2,1)} %pad_maximum_fusion.1), channel_id=1, source_target_pairs={{0,8},{2,10},{4,12},{6,14},{8,16},{10,18},{12,20},{14,22},{16,24},... | collective-permute-start | bytes 1572872 | tf_op jit(solution)/shard_map/ppermute | solution.py:15
  6.4 66.8 %collective-permute-start.3 = (bf16[2,256,512]{1,2,0:T(8,128)(2,1)}, bf16[2,256,512]{1,2,0:T(8,128)(2,1)}, u32[]{:S(2)}, u32[]{:S(2)}) collective-permute-start(bf16[2,256,512]{1,2,0:T(8,128)(2,1)} %pad_maximum_fusion.1), channel_id=1, source_target_pairs={{0,6},{2,8},{4,10},{6,12},{8,14},{10,16},{12,18},{14,20},{16,22},{... | collective-permute-start | bytes 1572872 | tf_op jit(solution)/shard_map/ppermute | solution.py:15
  10.5 64.6 %collective-permute-start.4 = (bf16[2,256,512]{1,2,0:T(8,128)(2,1)}, bf16[2,256,512]{1,2,0:T(8,128)(2,1)}, u32[]{:S(2)}, u32[]{:S(2)}) collective-permute-start(bf16[2,256,512]{1,2,0:T(8,128)(2,1)} %pad_maximum_fusion.1), channel_id=1, source_target_pairs={{0,4},{2,6},{4,8},{6,10},{8,12},{10,14},{12,16},{14,18},{16,20},{1... | collective-permute-start | bytes 1572872 | tf_op jit(solution)/shard_map/ppermute | solution.py:15
  12.4 44.2 %collective-permute-start = (bf16[2,256,512]{1,2,0:T(8,128)(2,1)}, bf16[2,256,512]{1,2,0:T(8,128)(2,1)}, u32[]{:S(2)}, u32[]{:S(2)}) collective-permute-start(bf16[2,256,512]{1,2,0:T(8,128)(2,1)} %pad_maximum_fusion.1), channel_id=1, source_target_pairs={{0,2},{2,4},{4,6},{6,8},{8,10},{10,12},{12,14},{14,16},{16,18},{18... | collective-permute-start | bytes 1572872 | tf_op jit(solution)/shard_map/ppermute | solution.py:15
  14.6 51.2 %collective-permute-start.1 = (bf16[2,256,512]{1,2,0:T(8,128)(2,1)}, bf16[2,256,512]{1,2,0:T(8,128)(2,1)S(1)}, u32[]{:S(2)}, u32[]{:S(2)}) collective-permute-start(bf16[2,256,512]{1,2,0:T(8,128)(2,1)} %pad_maximum_fusion.1), channel_id=1, source_target_pairs={{2,0},{4,2},{6,4},{8,6},{10,8},{12,10},{14,12},{16,14},{18,16},{20... | collective-permute-start | bytes 1572872 | tf_op jit(solution)/shard_map/ppermute | solution.py:15
  23.6 61.3 %collective-permute-start.5 = (bf16[2,256,512]{1,2,0:T(8,128)(2,1)}, bf16[2,256,512]{1,2,0:T(8,128)(2,1)}, u32[]{:S(2)}, u32[]{:S(2)}) collective-permute-start(bf16[2,256,512]{1,2,0:T(8,128)(2,1)} %pad_maximum_fusion.1), channel_id=1, source_target_pairs={{4,0},{6,2},{8,4},{10,6},{12,8},{14,10},{16,12},{18,14},{20,16},{2... | collective-permute-start | bytes 1572872 | tf_op jit(solution)/shard_map/ppermute | solution.py:15
  56.6 30.2 %collective-permute-start.6 = (bf16[2,256,512]{1,2,0:T(8,128)(2,1)}, bf16[2,256,512]{1,2,0:T(8,128)(2,1)}, u32[]{:S(2)}, u32[]{:S(2)}) collective-permute-start(bf16[2,256,512]{1,2,0:T(8,128)(2,1)} %pad_maximum_fusion.1), channel_id=1, source_target_pairs={{6,0},{8,2},{10,4},{12,6},{14,8},{16,10},{18,12},{20,14},{22,16},{... | collective-permute-start | bytes 1572872 | tf_op jit(solution)/shard_map/ppermute | solution.py:15
  65.8 11.3 %copy-start.3 = (bf16[2,256,512]{1,2,0:T(8,128)(2,1)}, bf16[2,256,512]{1,2,0:T(8,128)(2,1)S(1)}, u32[]{:S(2)}) copy-start(bf16[2,256,512]{1,2,0:T(8,128)(2,1)S(1)} %collective-permute-done.1) | copy-start | bytes 1572868
  65.8 23.0 %collective-permute-start.7 = (bf16[2,256,512]{1,2,0:T(8,128)(2,1)}, bf16[2,256,512]{1,2,0:T(8,128)(2,1)}, u32[]{:S(2)}, u32[]{:S(2)}) collective-permute-start(bf16[2,256,512]{1,2,0:T(8,128)(2,1)} %pad_maximum_fusion.1), channel_id=1, source_target_pairs={{8,0},{10,2},{12,4},{14,6},{16,8},{18,10},{20,12},{22,14},{24,16},... | collective-permute-start | bytes 1572872 | tf_op jit(solution)/shard_map/ppermute | solution.py:15
  81.6 2.5 %copy-start.4 = (bf16[2,256,512]{1,2,0:T(8,128)(2,1)S(1)}, bf16[2,256,512]{1,2,0:T(8,128)(2,1)}, u32[]{:S(2)}) copy-start(bf16[2,256,512]{1,2,0:T(8,128)(2,1)} %copy-done.3) | copy-start | bytes 1572868
  105.0 7.9 %copy-start.13 = (bf16[1,16,16,4,128]{4,3,2,1,0:T(4,128)(2,1)S(1)}, bf16[1,16,16,4,128]{4,3,2,1,0:T(4,128)(2,1)}, u32[]{:S(2)}) copy-start(bf16[1,16,16,4,128]{4,3,2,1,0:T(4,128)(2,1)} %reshape.466) | copy-start | bytes 786436
  112.9 2.2 %copy-start.1 = (bf16[2,144,16,4,128]{4,1,3,2,0:T(8,128)(2,1)}, bf16[2,144,16,4,128]{4,1,3,2,0:T(8,128)(2,1)S(1)}, u32[]{:S(2)}) copy-start(bf16[2,144,16,4,128]{4,1,3,2,0:T(8,128)(2,1)S(1)} %copy.88) | copy-start | bytes 14155780
  115.1 1.0 copy-start.7
  120.3 3.1 %copy-start.12 = (bf16[1,64,4,4,128]{4,3,2,1,0:T(4,128)(2,1)S(1)}, bf16[1,64,4,4,128]{4,3,2,1,0:T(4,128)(2,1)}, u32[]{:S(2)}) copy-start(bf16[1,64,4,4,128]{4,3,2,1,0:T(4,128)(2,1)} %reshape.464) | copy-start | bytes 786436
  120.3 3.1 %copy-start.15 = (pred[4,64,192]{2,1,0:T(8,128)(4,1)S(1)}, pred[4,64,192]{2,1,0:T(8,128)(4,1)}, u32[]{:S(2)}) copy-start(pred[4,64,192]{2,1,0:T(8,128)(4,1)} %and_and_fusion.1) | copy-start | bytes 147460
  122.1 1.2 copy-start.5
  124.0 1.1 copy-start.8
  125.5 2.9 %copy-start.6 = (bf16[2,192,4,4,128]{4,1,3,2,0:T(8,128)(2,1)S(1)}, bf16[2,192,4,4,128]{4,1,3,2,0:T(8,128)(2,1)}, u32[]{:S(2)}) copy-start(bf16[2,192,4,4,128]{4,1,3,2,0:T(8,128)(2,1)} %copy-done.5) | copy-start | bytes 4718596
  125.5 2.9 %copy-start.9 = (f32[4,4,64,192]{3,2,1,0:T(8,128)S(1)}, f32[4,4,64,192]{3,2,1,0:T(8,128)}, u32[]{:S(2)}) copy-start(f32[4,4,64,192]{3,2,1,0:T(8,128)} %copy-done.8) | copy-start | bytes 2359300
  128.4 2.5 %copy-start.14 = (pred[256,384]{0,1:T(8,128)(4,1)S(1)}, pred[256,384]{0,1:T(8,128)(4,1)}, u32[]{:S(2)}) copy-start(pred[256,384]{0,1:T(8,128)(4,1)} %fusion.18) | copy-start | bytes 294916
  130.9 1.8 %copy-start.10 = (bf16[2,384,1,4,128]{4,1,3,2,0:T(8,128)(2,1)S(1)}, bf16[2,384,1,4,128]{4,1,3,2,0:T(8,128)(2,1)}, u32[]{:S(2)}) copy-start(bf16[2,384,1,4,128]{4,1,3,2,0:T(8,128)(2,1)} %copy.51) | copy-start | bytes 2359300
  132.7 1.0 copy-start.11
where the time goes:
time: 141 us; the launch traced here: 140 us
  local copies, waits for them, and re-layouts  57 us (40%)
  waiting for transfers between devices  35 us (25%)
  starting transfers between devices  26.6 us (19%)
  matrix products  9.89 us (7%)
  other arithmetic  7.38 us (5%)
  blocking collectives  3.41 us (2%)
    ppermute x8, waiting for transfers between devices, from_behind(): lax.ppermute(value, axis, [(source, source + steps) for source in range(f...  35 us
    ppermute x8, starting transfers between devices, from_behind(): lax.ppermute(value, axis, [(source, source + steps) for source in range(f...  26.6 us
    reshape x5, local copies, waits for them, and re-layouts, band_scores(): window_keys.reshape(2, residue_rows + 2 * SIDE_KEY_COUNT, dilation_step,...  22.1 us
    unnamed x41, local copies, waits for them, and re-layouts  18.4 us
    concatenate x3, local copies, waits for them, and re-layouts, per_device(): extended = jnp.concatenate(far_blocks(stacked_groups, hop_count), axis=1)  11.2 us
    dot_general x3, matrix products, one_block(): jnp.einsum('rhqk,rhke->rhqe', weights, laid[1], preferred_element_type=jn...  4.69 us
    dot_general x3, matrix products, one_block(): jnp.einsum('rhqe,rhke->rhqk', query_block, laid[0], preferred_element_typ...  3.68 us
    all_gather x1, blocking collectives, per_device(): lax.all_gather(attended, 'tp', axis=1, tiled=True)  3.41 us
  transfers between devices with their start and end apart: 8, of which 2 were waited for; matrix products, arithmetic and copies ran while one was open for 17% of the time, Pallas kernels for 0%

commit v1 on v0

v1 whole, which is shorter than its diff:
```python
import functools
import math

import jax
import jax.numpy as jnp
from jax import lax
from jax.experimental import pallas as pl
from jax.experimental.pallas import tpu as pltpu
from jax.sharding import PartitionSpec as P

HEAD_DIM = 128
SIDE = 64
MID = 4
FAR = 16
MESH = pl.DeviceIdType.MESH
F32 = jnp.float32
BF16 = jnp.bfloat16
SCALE = HEAD_DIM ** -0.5 * math.log2(math.e)


def nt(a, b):
    return lax.dot_general(a, b, (((1,), (1,)), ((), ())), preferred_element_type=F32)


def nn(a, b):
    return lax.dot_general(a, b, (((1,), (0,)), ((), ())), preferred_element_type=F32)


def iota(shape, dim):
    return lax.broadcasted_iota(jnp.int32, shape, dim)


def attend(q, k, v, allowed):
    s = jnp.where(allowed, nt(q, k) * SCALE, -jnp.inf)
    top = jnp.max(s, axis=-1, keepdims=True)
    raised = jnp.exp2(s - top)
    den = jnp.sum(raised, axis=-1, keepdims=True)
    return nn(raised.astype(BF16), v), top, den


def kernel(sp_n, heads, q_hbm, k_hbm, v_hbm, w_hbm, out_ref,
           q_in, k_in, v_in, w, pq, pkv, qf, kvf, near_lo, near_hi, ob, ret, att, att_other, acc_n, md_n,
           load_sem, kv_s, kv_r, q_s, q_r, up_s, up_r, dn_s, dn_r, near_s, near_r, ret_s, ret_r, tp_s, tp_r):
    rows = q_in.shape[0]
    chunk = rows // MID
    mm = rows // FAR
    e = HEAD_DIM
    p, c = lax.axis_index("sp"), lax.axis_index("tp")
    groups = sp_n // MID
    g, j = p // MID, p % MID

    loads = [
        pltpu.make_async_copy(src, dst, load_sem.at[n])
        for n, (src, dst) in enumerate(((k_hbm, k_in), (v_hbm, v_in), (q_hbm, q_in), (w_hbm, w)))
    ]
    for load in loads:
        load.start()

    barrier = pltpu.get_barrier_semaphore()

    def greet(sp, tp):
        pl.semaphore_signal(barrier, inc=1, device_id=(sp, tp), device_id_type=MESH)

    def mate(d):
        return g * MID + (j + d) % MID

    for d in range(1, MID):
        greet(mate(d), c)
    greet(p, 1 - c)
    has_dn, has_up = g > 0, g < groups - 1
    has_prev, has_next = p > 0, p < sp_n - 1

    @pl.when(has_dn)
    def _():
        greet(p - MID, c)

    @pl.when(has_up)
    def _():
        greet(p + MID, c)

    @pl.when(has_prev)
    def _():
        greet(p - 1, c)

    @pl.when(has_next)
    def _():
        greet(p + 1, c)

    def remote(src, dst, ss, rs, sp, tp):
        return pltpu.make_async_remote_copy(
            src_ref=src, dst_ref=dst, send_sem=ss, recv_sem=rs, device_id=(sp, tp), device_id_type=MESH)

    r, t = iota((rows, rows), 0), iota((rows, rows), 1)
    perm = (t == FAR * (r % mm) + MID * ((r % chunk) // mm) + r // chunk).astype(BF16)
    r, t = t, r
    back = (t == FAR * (r % mm) + MID * ((r % chunk) // mm) + r // chunk).astype(BF16)

    loads[0].wait()
    loads[1].wait()
    pk = nn(perm, k_in[...]).astype(BF16)
    pv = nn(perm, v_in[...]).astype(BF16)
    for h in range(heads):
        pkv[h, 0] = pk[:, h * e:(h + 1) * e]
        pkv[h, 1] = pv[:, h * e:(h + 1) * e]

    def at(n, base=0):
        return pl.ds(pl.multiple_of(base + n * chunk, chunk), chunk)

    for h in range(heads):
        for n in range(2):
            kvf[h, n, at(j, rows), :] = pkv[h, n, at(j), :]

    def edge(test, rows_at, near):
        @pl.when(jnp.logical_not(test))
        def _():
            for h in range(heads):
                for n in range(2):
                    kvf[h, n, pl.ds(rows_at, rows), :] = jnp.zeros((rows, e), BF16)

    edge(has_dn, 0, near_lo)
    edge(has_up, 2 * rows, near_hi)

    @pl.when(jnp.logical_not(has_prev))
    def _():
        near_lo[...] = jnp.zeros_like(near_lo)

    @pl.when(jnp.logical_not(has_next))
    def _():
        near_hi[...] = jnp.zeros_like(near_hi)

    pl.semaphore_wait(
        barrier,
        MID + has_dn.astype(jnp.int32) + has_up.astype(jnp.int32)
        + has_prev.astype(jnp.int32) + has_next.astype(jnp.int32))

    def up(h, d):
        n = (j - d + MID) % MID
        src = pkv.at[h, :, at(n), :] if d == 0 else kvf.at[h, :, at(n, rows), :]
        return remote(src, kvf.at[h, :, at(n), :], up_s.at[h, d], up_r.at[h, d], (p + MID) % sp_n, c)

    def down(h, d):
        n = (j - d + MID) % MID
        src = pkv.at[h, :, at(n), :] if d == 0 else kvf.at[h, :, at(n, rows), :]
        return remote(src, kvf.at[h, :, at(n, 2 * rows), :], dn_s.at[h, d], dn_r.at[h, d], (p - MID + sp_n) % sp_n, c)

    def forward(h, d):
        @pl.when(has_up)
        def _():
            up(h, d).start()

        @pl.when(has_dn)
        def _():
            down(h, d).start()

    def kv(h, d, receive=False):
        dst = (j - d + MID) % MID if receive else j
        return remote(pkv.at[h, :, at((j + d) % MID), :], kvf.at[h, :, at(dst, rows), :],
                      kv_s.at[h, d - 1], kv_r.at[h, d - 1], mate(d), c)

    def queries(d, receive=False):
        dst = (j - d + MID) % MID if receive else j
        return remote(pq.at[:, at((j + d) % MID), :], qf.at[:, at(dst), :],
                      q_s.at[d - 1], q_r.at[d - 1], mate(d), c)

    for h in range(heads):
        for d in range(1, MID):
            kv(h, d).start()
        forward(h, 0)

    loads[2].wait()
    pq_all = nn(perm, q_in[...]).astype(BF16)
    for h in range(heads):
        pq[h] = pq_all[:, h * e:(h + 1) * e]
    for h in range(heads):
        qf[h, at(j), :] = pq[h, at(j), :]
    for d in range(1, MID):
        queries(d).start()

    def near(n, to_next):
        src = (k_in, v_in)[n]
        if to_next:
            return remote(src.at[pl.ds(rows - SIDE, SIDE), :], near_lo.at[n],
                          near_s.at[n, 0], near_r.at[n, 0], (p + 1) % sp_n, c)
        return remote(src.at[pl.ds(0, SIDE), :], near_hi.at[n],
                      near_s.at[n, 1], near_r.at[n, 1], (p - 1 + sp_n) % sp_n, c)

    @pl.when(has_next)
    def _():
        for n in range(2):
            near(n, True).start()

    @pl.when(has_prev)
    def _():
        for n in range(2):
            near(n, False).start()

    for h in range(heads):
        for d in range(1, MID):
            kv(h, d, receive=True).wait_recv()
            forward(h, d)

    @pl.when(has_prev)
    def _():
        for n in range(2):
            near(n, True).wait_recv()

    @pl.when(has_next)
    def _():
        for n in range(2):
            near(n, False).wait_recv()

    half = rows // 2
    span = half + 2 * SIDE
    qi, ki = iota((half, span), 0), iota((half, span), 1)
    band = (ki >= qi) & (ki <= qi + 2 * SIDE)
    lo_ok, hi_ok = has_prev.astype(jnp.int32), has_next.astype(jnp.int32)
    allowed = (band & ((ki >= SIDE) | (lo_ok == 1)), band & ((ki < span - SIDE) | (hi_ok == 1)))
    for h in range(heads):
        cols = slice(h * e, (h + 1) * e)
        ks = [jnp.concatenate([near_lo[n, :, cols], x[:, cols], near_hi[n, :, cols]], axis=0)
              for n, x in enumerate((k_in, v_in))]
        for b in range(2):
            at_b = slice(b * half, (b + 1) * half)
            o, top, den = attend(q_in[at_b, cols], ks[0][b * half:b * half + span],
                                 ks[1][b * half:b * half + span], allowed[b])
            acc_n[h, at_b, :] = o
            md_n[h, 0, at_b, :] = jnp.broadcast_to(top, (half, e))
            md_n[h, 1, at_b, :] = jnp.broadcast_to(den, (half, e))

    for d in range(1, MID):
        queries(d, receive=True).wait_recv()

    def order(x):
        return chunk * (x // chunk) + (FAR // MID) * (x % mm) + (x % chunk) // mm

    dn_ok, up_ok = has_dn.astype(jnp.int32), has_up.astype(jnp.int32)
    gap = order(ki) - order(qi)
    band = (gap >= 0) & (gap <= 2 * SIDE)
    mid_ok = (band & ((ki >= SIDE) | (dn_ok == 1)), band & ((ki < span - SIDE) | (up_ok == 1)))
    far_span = 3 * chunk
    qi, ki = iota((chunk, far_span), 0), iota((chunk, far_span), 1)
    far_ok = ((ki >= qi) & (ki <= qi + 2 * SIDE) & ((ki >= chunk) | (dn_ok == 1))
              & ((ki < 2 * chunk) | (up_ok == 1)))
    lane = iota((rows, e), 1)

    def result(h, d, receive=False):
        dst = (j - d + MID) % MID if receive else j
        return remote(ob.at[h, :, at((j + d) % MID), :], ret.at[h, :, at(dst), :],
                      ret_s.at[h, d - 1], ret_r.at[h, d - 1], mate(d), c)

    for h in range(heads):
        @pl.when(has_dn)
        def _():
            for d in range(MID):
                up(h, d).wait_recv()

        @pl.when(has_up)
        def _():
            for d in range(MID):
                down(h, d).wait_recv()

        q = qf[h]
        kh, vh = kvf[h, 0], kvf[h, 1]
        mids = []
        for b in range(2):
            first = rows - chunk + b * half
            mids.append(attend(q[b * half:(b + 1) * half], kh[first:first + span], vh[first:first + span], mid_ok[b]))
        o1, t1, d1 = (jnp.concatenate([mids[0][n], mids[1][n]], axis=0) for n in range(3))
        q4 = q.reshape(MID, FAR // MID, mm, e)
        k4 = kh.reshape(3 * MID, FAR // MID, mm, e)
        v4 = vh.reshape(3 * MID, FAR // MID, mm, e)
        fars = [
            attend(q4[:, s].reshape(chunk, e), k4[:, s].reshape(far_span, e), v4[:, s].reshape(far_span, e), far_ok)
            for s in range(FAR // MID)
        ]
        o2, t2, d2 = (
            jnp.concatenate(
                [fars[s][n][i * mm:(i + 1) * mm] for i in range(MID) for s in range(FAR // MID)], axis=0)
            for n in range(3))
        top = jnp.maximum(t1, t2)
        e1, e2 = jnp.exp2(t1 - top), jnp.exp2(t2 - top)
        den = e1 * d1 + e2 * d2
        ob[h, 0] = ((e1 * o1 + e2 * o2) / den).astype(BF16)
        log_den = jnp.broadcast_to(top + jnp.log2(den), (rows, e))
        one = log_den.astype(BF16).astype(F32)
        two = (log_den - one).astype(BF16).astype(F32)
        three = log_den - one - two
        ob[h, 1] = jnp.where(lane == 0, one, jnp.where(lane == 1, two, three)).astype(BF16)
        for d in range(1, MID):
            result(h, d).start()
        for n in range(2):
            ret[h, n, at(j), :] = ob[h, n, at(j), :]

    def share(h):
        cols = pl.ds(h * e, e)
        return remote(att.at[:, cols], att_other.at[:, cols], tp_s.at[h], tp_r.at[h], p, 1 - c)

    for h in range(heads):
        for d in range(1, MID):
            result(h, d, receive=True).wait_recv()
        both = nn(back, jnp.concatenate([ret[h, 0], ret[h, 1]], axis=1))
        o, parts = both[:, :e], both[:, e:]
        log_den = parts[:, 0:1] + parts[:, 1:2] + parts[:, 2:3]
        t_n, d_n = md_n[h, 0], md_n[h, 1]
        top = jnp.maximum(t_n, log_den)
        e1, e2 = jnp.exp2(t_n - top), jnp.exp2(log_den - top)
        att[:, h * e:(h + 1) * e] = ((e1 * acc_n[h] + e2 * o) / (e1 * d_n + e2)).astype(BF16)
        share(h).start()

    width = heads * e
    loads[3].wait()
    own = nn(att[...], w[pl.ds(pl.multiple_of(c * width, width), width), :])
    for h in range(heads):
        share(h).wait_recv()
    other = nn(att_other[...], w[pl.ds(pl.multiple_of((1 - c) * width, width), width), :])
    out_ref[...] = (own + other).astype(BF16)

    for h in range(heads):
        for d in range(1, MID):
            kv(h, d).wait_send()
            result(h, d).wait_send()
        share(h).wait_send()
    for d in range(1, MID):
        queries(d).wait_send()

    @pl.when(has_up)
    def _():
        for h in range(heads):
            for d in range(MID):
                up(h, d).wait_send()

    @pl.when(has_dn)
    def _():
        for h in range(heads):
            for d in range(MID):
                down(h, d).wait_send()

    @pl.when(has_next)
    def _():
        for n in range(2):
            near(n, True).wait_send()

    @pl.when(has_prev)
    def _():
        for n in range(2):
            near(n, False).wait_send()


def per_device(sp_n, q, k, v, w):
    rows, columns = q.shape
    heads = columns // HEAD_DIM
    assert MID * rows == SIDE * FAR and rows // MID == SIDE and sp_n % MID == 0
    dma = pltpu.SemaphoreType.DMA
    e = HEAD_DIM
    return pl.pallas_call(
        functools.partial(kernel, sp_n, heads),
        out_shape=jax.ShapeDtypeStruct((rows, w.shape[1]), BF16),
        in_specs=[pl.BlockSpec(memory_space=pl.ANY)] * 4,
        out_specs=pl.BlockSpec(memory_space=pltpu.VMEM),
        scratch_shapes=[
            pltpu.VMEM((rows, columns), BF16),
            pltpu.VMEM((rows, columns), BF16),
            pltpu.VMEM((rows, columns), BF16),
            pltpu.VMEM(w.shape, BF16),
            pltpu.VMEM((heads, rows, e), BF16),
            pltpu.VMEM((heads, 2, rows, e), BF16),
            pltpu.VMEM((heads, rows, e), BF16),
            pltpu.VMEM((heads, 2, 3 * rows, e), BF16),
            pltpu.VMEM((2, SIDE, columns), BF16),
            pltpu.VMEM((2, SIDE, columns), BF16),
            pltpu.VMEM((heads, 2, rows, e), BF16),
            pltpu.VMEM((heads, 2, rows, e), BF16),
            pltpu.VMEM((rows, columns), BF16),
            pltpu.VMEM((rows, columns), BF16),
            pltpu.VMEM((heads, rows, e), F32),
            pltpu.VMEM((heads, 2, rows, e), F32),
            dma((4,)),
            dma((heads, MID - 1)), dma((heads, MID - 1)),
            dma((MID - 1,)), dma((MID - 1,)),
            dma((heads, MID)), dma((heads, MID)),
            dma((heads, MID)), dma((heads, MID)),
            dma((2, 2)), dma((2, 2)),
            dma((heads, MID - 1)), dma((heads, MID - 1)),
            dma((heads,)), dma((heads,)),
        ],
        compiler_params=pltpu.CompilerParams(collective_id=0, has_side_effects=True),
    )(q, k, v, w)


def solution(mesh):
    return jax.shard_map(
        functools.partial(per_device, mesh.shape["sp"]), mesh=mesh,
        in_specs=(P("sp", "tp"), P("sp", "tp"), P("sp", "tp"), P(None, "tp")),
        out_specs=P("sp", "tp"), check_vma=False,
    )
```

time: 141 us -> 36.1 us (0.26)
  the two profiles are of different devices: /device:TPU:17 before, /device:TPU:1 now
where the time goes in v1:
time: 36.1 us; the launch traced here: 35.9 us
  Pallas kernels  34 us (94%)
  local copies, waits for them, and re-layouts  1.87 us (5%)
    pallas_call x1, Pallas kernels, per_device(): pl.pallas_call(functools.partial(kernel, sp_n, heads), out_shape=jax.Shap...  34 us
    unnamed x1, local copies, waits for them, and re-layouts  1.87 us

profile of v1, /device:TPU:1, one launch (start us, length us, event | category | flops | bytes accessed | tf_op | source)
XLA Modules:
  0.0 35.9 jit_solution(7275721495213839807)
XLA Ops:
  0.0 34.0 %shard_map.46 = bf16[256,1024]{1,0:T(8,128)(2,1)} custom-call(bf16[256,512]{1,0:T(8,128)(2,1)} %q_hbm.1, bf16[256,512]{1,0:T(8,128)(2,1)} %k_hbm.1, bf16[256,512]{1,0:T(8,128)(2,1)} %v_hbm.1, bf16[1024,1024]{1,0:T(8,128)(2,1)} %w_hbm.1), custom_call_target="tpu_custom_call" | custom-call | tf_op jit(solution)/shard_map/pallas_call | solution.py:355
  34.0 1.9 %copy.6 = bf16[256,1024]{1,0:T(8,128)(2,1)} copy(bf16[256,1024]{1,0:T(8,128)(2,1)} %shard_map.46) | data formatting | bytes 1048576

commit v2 on v1

--- a/solution.py
+++ b/solution.py
@@ -39,8 +39,8 @@
 
 
 def kernel(sp_n, heads, q_hbm, k_hbm, v_hbm, w_hbm, out_ref,
-           q_in, k_in, v_in, w, pq, pkv, qf, kvf, near_lo, near_hi, ob, ret, att, att_other, acc_n, md_n,
-           load_sem, kv_s, kv_r, q_s, q_r, up_s, up_r, dn_s, dn_r, near_s, near_r, ret_s, ret_r, tp_s, tp_r):
+           q_in, k_in, v_in, w, pkv, kvf, near_lo, near_hi, ob, ret, att, att_other, acc_n, md_n,
+           load_sem, kv_s, kv_r, up_s, up_r, dn_s, dn_r, near_s, near_r, ret_s, ret_r, tp_s, tp_r):
     rows = q_in.shape[0]
     chunk = rows // MID
     mm = rows // FAR
@@ -95,30 +95,28 @@
     r, t = t, r
     back = (t == FAR * (r % mm) + MID * ((r % chunk) // mm) + r // chunk).astype(BF16)
 
-    loads[0].wait()
-    loads[1].wait()
-    pk = nn(perm, k_in[...]).astype(BF16)
-    pv = nn(perm, v_in[...]).astype(BF16)
-    for h in range(heads):
-        pkv[h, 0] = pk[:, h * e:(h + 1) * e]
-        pkv[h, 1] = pv[:, h * e:(h + 1) * e]
+    for n, x in enumerate((k_in, v_in, q_in)):
+        loads[n].wait()
+        moved = nn(perm, x[...]).astype(BF16)
+        for h in range(heads):
+            pkv[h, n] = moved[:, h * e:(h + 1) * e]
 
     def at(n, base=0):
         return pl.ds(pl.multiple_of(base + n * chunk, chunk), chunk)
 
     for h in range(heads):
-        for n in range(2):
+        for n in range(3):
             kvf[h, n, at(j, rows), :] = pkv[h, n, at(j), :]
 
-    def edge(test, rows_at, near):
+    def edge(test, rows_at):
         @pl.when(jnp.logical_not(test))
         def _():
             for h in range(heads):
                 for n in range(2):
                     kvf[h, n, pl.ds(rows_at, rows), :] = jnp.zeros((rows, e), BF16)
 
-    edge(has_dn, 0, near_lo)
-    edge(has_up, 2 * rows, near_hi)
+    edge(has_dn, 0)
+    edge(has_up, 2 * rows)
 
     @pl.when(jnp.logical_not(has_prev))
     def _():
@@ -135,13 +133,13 @@
 
     def up(h, d):
         n = (j - d + MID) % MID
-        src = pkv.at[h, :, at(n), :] if d == 0 else kvf.at[h, :, at(n, rows), :]
-        return remote(src, kvf.at[h, :, at(n), :], up_s.at[h, d], up_r.at[h, d], (p + MID) % sp_n, c)
+        src = pkv.at[h, 0:2, at(n), :] if d == 0 else kvf.at[h, 0:2, at(n, rows), :]
+        return remote(src, kvf.at[h, 0:2, at(n), :], up_s.at[h, d], up_r.at[h, d], (p + MID) % sp_n, c)
 
     def down(h, d):
         n = (j - d + MID) % MID
-        src = pkv.at[h, :, at(n), :] if d == 0 else kvf.at[h, :, at(n, rows), :]
-        return remote(src, kvf.at[h, :, at(n, 2 * rows), :], dn_s.at[h, d], dn_r.at[h, d], (p - MID + sp_n) % sp_n, c)
+        src = pkv.at[h, 0:2, at(n), :] if d == 0 else kvf.at[h, 0:2, at(n, rows), :]
+        return remote(src, kvf.at[h, 0:2, at(n, 2 * rows), :], dn_s.at[h, d], dn_r.at[h, d], (p - MID + sp_n) % sp_n, c)
 
     def forward(h, d):
         @pl.when(has_up)
@@ -157,24 +155,10 @@
         return remote(pkv.at[h, :, at((j + d) % MID), :], kvf.at[h, :, at(dst, rows), :],
                       kv_s.at[h, d - 1], kv_r.at[h, d - 1], mate(d), c)
 
-    def queries(d, receive=False):
-        dst = (j - d + MID) % MID if receive else j
-        return remote(pq.at[:, at((j + d) % MID), :], qf.at[:, at(dst), :],
-                      q_s.at[d - 1], q_r.at[d - 1], mate(d), c)
-
     for h in range(heads):
         for d in range(1, MID):
             kv(h, d).start()
         forward(h, 0)
-
-    loads[2].wait()
-    pq_all = nn(perm, q_in[...]).astype(BF16)
-    for h in range(heads):
-        pq[h] = pq_all[:, h * e:(h + 1) * e]
-    for h in range(heads):
-        qf[h, at(j), :] = pq[h, at(j), :]
-    for d in range(1, MID):
-        queries(d).start()
 
     def near(n, to_next):
         src = (k_in, v_in)[n]
@@ -199,36 +183,9 @@
             kv(h, d, receive=True).wait_recv()
             forward(h, d)
 
-    @pl.when(has_prev)
-    def _():
-        for n in range(2):
-            near(n, True).wait_recv()
-
-    @pl.when(has_next)
-    def _():
-        for n in range(2):
-            near(n, False).wait_recv()
-
     half = rows // 2
     span = half + 2 * SIDE
     qi, ki = iota((half, span), 0), iota((half, span), 1)
-    band = (ki >= qi) & (ki <= qi + 2 * SIDE)
-    lo_ok, hi_ok = has_prev.astype(jnp.int32), has_next.astype(jnp.int32)
-    allowed = (band & ((ki >= SIDE) | (lo_ok == 1)), band & ((ki < span - SIDE) | (hi_ok == 1)))
-    for h in range(heads):
-        cols = slice(h * e, (h + 1) * e)
-        ks = [jnp.concatenate([near_lo[n, :, cols], x[:, cols], near_hi[n, :, cols]], axis=0)
-              for n, x in enumerate((k_in, v_in))]
-        for b in range(2):
-            at_b = slice(b * half, (b + 1) * half)
-            o, top, den = attend(q_in[at_b, cols], ks[0][b * half:b * half + span],
-                                 ks[1][b * half:b * half + span], allowed[b])
-            acc_n[h, at_b, :] = o
-            md_n[h, 0, at_b, :] = jnp.broadcast_to(top, (half, e))
-            md_n[h, 1, at_b, :] = jnp.broadcast_to(den, (half, e))
-
-    for d in range(1, MID):
-        queries(d, receive=True).wait_recv()
 
     def order(x):
         return chunk * (x // chunk) + (FAR // MID) * (x % mm) + (x % chunk) // mm
@@ -242,10 +199,11 @@
     far_ok = ((ki >= qi) & (ki <= qi + 2 * SIDE) & ((ki >= chunk) | (dn_ok == 1))
               & ((ki < 2 * chunk) | (up_ok == 1)))
     lane = iota((rows, e), 1)
+    pick = (iota((16, e), 0) == iota((16, e), 1)).astype(BF16)
 
     def result(h, d, receive=False):
         dst = (j - d + MID) % MID if receive else j
-        return remote(ob.at[h, :, at((j + d) % MID), :], ret.at[h, :, at(dst), :],
+        return remote(ob.at[h, (j + d) % MID], ret.at[h, dst],
                       ret_s.at[h, d - 1], ret_r.at[h, d - 1], mate(d), c)
 
     for h in range(heads):
@@ -259,7 +217,7 @@
             for d in range(MID):
                 down(h, d).wait_recv()
 
-        q = qf[h]
+        q = kvf[h, 2, pl.ds(rows, rows), :]
         kh, vh = kvf[h, 0], kvf[h, 1]
         mids = []
         for b in range(2):
@@ -280,16 +238,51 @@
         top = jnp.maximum(t1, t2)
         e1, e2 = jnp.exp2(t1 - top), jnp.exp2(t2 - top)
         den = e1 * d1 + e2 * d2
-        ob[h, 0] = ((e1 * o1 + e2 * o2) / den).astype(BF16)
+        o = ((e1 * o1 + e2 * o2) / den).astype(BF16)
         log_den = jnp.broadcast_to(top + jnp.log2(den), (rows, e))
         one = log_den.astype(BF16).astype(F32)
         two = (log_den - one).astype(BF16).astype(F32)
         three = log_den - one - two
-        ob[h, 1] = jnp.where(lane == 0, one, jnp.where(lane == 1, two, three)).astype(BF16)
+        parts = jnp.where(lane == 0, one, jnp.where(lane == 1, two, three)).astype(BF16)
+        twice = [parts[i * chunk:(i + 1) * chunk] for i in range(MID) for _ in range(2)]
+        flat = nt(pick, jnp.concatenate(twice, axis=0)).astype(BF16)
+        for i in range(MID):
+            ob[h, i, :chunk] = o[i * chunk:(i + 1) * chunk]
+            ob[h, i, chunk:] = flat[:, 2 * i * chunk:2 * (i + 1) * chunk]
         for d in range(1, MID):
             result(h, d).start()
-        for n in range(2):
-            ret[h, n, at(j), :] = ob[h, n, at(j), :]
+        ret[h, pl.ds(j, 1)] = ob[h, pl.ds(j, 1)]
+
+    @pl.when(has_prev)
+    def _():
+        for n in range(2):
+            near(n, True).wait_recv()
+
+    @pl.when(has_next)
+    def _():
+        for n in range(2):
+            near(n, False).wait_recv()
+
+    qi, ki = iota((half, span), 0), iota((half, span), 1)
+    band = (ki >= qi) & (ki <= qi + 2 * SIDE)
+    lo_ok, hi_ok = has_prev.astype(jnp.int32), has_next.astype(jnp.int32)
+    allowed = (band & ((ki >= SIDE) | (lo_ok == 1)), band & ((ki < span - SIDE) | (hi_ok == 1)))
+    for h in range(heads):
+        cols = slice(h * e, (h + 1) * e)
+        ks = [jnp.concatenate([near_lo[n, :, cols], x[:, cols], near_hi[n, :, cols]], axis=0)
+              for n, x in enumerate((k_in, v_in))]
+        for b in range(2):
+            at_b = slice(b * half, (b + 1) * half)
+            o, top, den = attend(q_in[at_b, cols], ks[0][b * half:b * half + span],
+                                 ks[1][b * half:b * half + span], allowed[b])
+            acc_n[h, at_b, :] = o
+            md_n[h, 0, at_b, :] = jnp.broadcast_to(top, (half, e))
+            md_n[h, 1, at_b, :] = jnp.broadcast_to(den, (half, e))
+
+    r, t = iota((rows, 2 * rows), 1), iota((rows, 2 * rows), 0)
+    low = r % (2 * chunk) < chunk
+    r = r // (2 * chunk) * chunk + r % (2 * chunk)
+    back_twice = (low & (t == FAR * (r % mm) + MID * ((r % chunk) // mm) + r // chunk)).astype(BF16)
 
     def share(h):
         cols = pl.ds(h * e, e)
@@ -298,8 +291,8 @@
     for h in range(heads):
         for d in range(1, MID):
             result(h, d, receive=True).wait_recv()
-        both = nn(back, jnp.concatenate([ret[h, 0], ret[h, 1]], axis=1))
-        o, parts = both[:, :e], both[:, e:]
+        o = nn(back, jnp.concatenate([ret[h, i, :chunk] for i in range(MID)], axis=0))
+        parts = nt(back_twice, jnp.concatenate([ret[h, i, chunk:] for i in range(MID)], axis=1))
         log_den = parts[:, 0:1] + parts[:, 1:2] + parts[:, 2:3]
         t_n, d_n = md_n[h, 0], md_n[h, 1]
         top = jnp.maximum(t_n, log_den)
@@ -320,9 +313,6 @@
             kv(h, d).wait_send()
             result(h, d).wait_send()
         share(h).wait_send()
-    for d in range(1, MID):
-        queries(d).wait_send()
-
     @pl.when(has_up)
     def _():
         for h in range(heads):
@@ -351,7 +341,7 @@
     heads = columns // HEAD_DIM
     assert MID * rows == SIDE * FAR and rows // MID == SIDE and sp_n % MID == 0
     dma = pltpu.SemaphoreType.DMA
-    e = HEAD_DIM
+    e, chunk = HEAD_DIM, rows // MID
     return pl.pallas_call(
         functools.partial(kernel, sp_n, heads),
         out_shape=jax.ShapeDtypeStruct((rows, w.shape[1]), BF16),
@@ -362,21 +352,18 @@
             pltpu.VMEM((rows, columns), BF16),
             pltpu.VMEM((rows, columns), BF16),
             pltpu.VMEM(w.shape, BF16),
-            pltpu.VMEM((heads, rows, e), BF16),
-            pltpu.VMEM((heads, 2, rows, e), BF16),
-            pltpu.VMEM((heads, rows, e), BF16),
-            pltpu.VMEM((heads, 2, 3 * rows, e), BF16),
+            pltpu.VMEM((heads, 3, rows, e), BF16),
+            pltpu.VMEM((heads, 3, 3 * rows, e), BF16),
             pltpu.VMEM((2, SIDE, columns), BF16),
             pltpu.VMEM((2, SIDE, columns), BF16),
-            pltpu.VMEM((heads, 2, rows, e), BF16),
-            pltpu.VMEM((heads, 2, rows, e), BF16),
+            pltpu.VMEM((heads, MID, chunk + 16, e), BF16),
+            pltpu.VMEM((heads, MID, chunk + 16, e), BF16),
             pltpu.VMEM((rows, columns), BF16),
             pltpu.VMEM((rows, columns), BF16),
             pltpu.VMEM((heads, rows, e), F32),
             pltpu.VMEM((heads, 2, rows, e), F32),
             dma((4,)),
             dma((heads, MID - 1)), dma((heads, MID - 1)),
-            dma((MID - 1,)), dma((MID - 1,)),
             dma((heads, MID)), dma((heads, MID)),
             dma((heads, MID)), dma((heads, MID)),
             dma((2, 2)), dma((2, 2)),

time: 36.1 us -> 34.5 us (0.956)
  Pallas kernels: 34 us -> 32.4 us
    pallas_call x1, Pallas kernels: 34 us -> 32.4 us  [per_device(): pl.pallas_call(functools.partial(kernel, sp_n, heads), out_shape=jax.Shap...]
where the time goes in v2:
time: 34.5 us; the launch traced here: 34.3 us
  Pallas kernels  32.4 us (94%)
  local copies, waits for them, and re-layouts  1.87 us (5%)
    pallas_call x1, Pallas kernels, per_device(): pl.pallas_call(functools.partial(kernel, sp_n, heads), out_shape=jax.Shap...  32.4 us
    unnamed x1, local copies, waits for them, and re-layouts  1.87 us

profile of v2, /device:TPU:1, one launch (start us, length us, event | category | flops | bytes accessed | tf_op | source)
XLA Modules:
  0.0 34.3 jit_solution(3643951188764136448)
XLA Ops:
  0.0 32.4 %shard_map.46 = bf16[256,1024]{1,0:T(8,128)(2,1)} custom-call(bf16[256,512]{1,0:T(8,128)(2,1)} %q_hbm.1, bf16[256,512]{1,0:T(8,128)(2,1)} %k_hbm.1, bf16[256,512]{1,0:T(8,128)(2,1)} %v_hbm.1, bf16[1024,1024]{1,0:T(8,128)(2,1)} %w_hbm.1), custom_call_target="tpu_custom_call" | custom-call | tf_op jit(solution)/shard_map/pallas_call | solution.py:345
  32.4 1.9 %copy.6 = bf16[256,1024]{1,0:T(8,128)(2,1)} copy(bf16[256,1024]{1,0:T(8,128)(2,1)} %shard_map.46) | data formatting | bytes 1048576

commit v3 on v2

--- a/solution.py
+++ b/solution.py
@@ -40,7 +40,7 @@
 
 def kernel(sp_n, heads, q_hbm, k_hbm, v_hbm, w_hbm, out_ref,
            q_in, k_in, v_in, w, pkv, kvf, near_lo, near_hi, ob, ret, att, att_other, acc_n, md_n,
-           load_sem, kv_s, kv_r, up_s, up_r, dn_s, dn_r, near_s, near_r, ret_s, ret_r, tp_s, tp_r):
+           load_sem, kv_s, kv_r, q_s, q_r, up_s, up_r, dn_s, dn_r, near_s, near_r, ret_s, ret_r, tp_s, tp_r):
     rows = q_in.shape[0]
     chunk = rows // MID
     mm = rows // FAR
@@ -152,13 +152,20 @@
 
     def kv(h, d, receive=False):
         dst = (j - d + MID) % MID if receive else j
-        return remote(pkv.at[h, :, at((j + d) % MID), :], kvf.at[h, :, at(dst, rows), :],
+        return remote(pkv.at[h, 0:2, at((j + d) % MID), :], kvf.at[h, 0:2, at(dst, rows), :],
                       kv_s.at[h, d - 1], kv_r.at[h, d - 1], mate(d), c)
+
+    def queries(d, receive=False):
+        dst = (j - d + MID) % MID if receive else j
+        return remote(pkv.at[:, 2, at((j + d) % MID), :], kvf.at[:, 2, at(dst, rows), :],
+                      q_s.at[d - 1], q_r.at[d - 1], mate(d), c)
 
     for h in range(heads):
         for d in range(1, MID):
             kv(h, d).start()
         forward(h, 0)
+    for d in range(1, MID):
+        queries(d).start()
 
     def near(n, to_next):
         src = (k_in, v_in)[n]
@@ -199,6 +206,8 @@
     far_ok = ((ki >= qi) & (ki <= qi + 2 * SIDE) & ((ki >= chunk) | (dn_ok == 1))
               & ((ki < 2 * chunk) | (up_ok == 1)))
     lane = iota((rows, e), 1)
+    for d in range(1, MID):
+        queries(d, receive=True).wait_recv()
     pick = (iota((16, e), 0) == iota((16, e), 1)).astype(BF16)
 
     def result(h, d, receive=False):
@@ -313,6 +322,8 @@
             kv(h, d).wait_send()
             result(h, d).wait_send()
         share(h).wait_send()
+    for d in range(1, MID):
+        queries(d).wait_send()
     @pl.when(has_up)
     def _():
         for h in range(heads):
@@ -364,6 +375,7 @@
             pltpu.VMEM((heads, 2, rows, e), F32),
             dma((4,)),
             dma((heads, MID - 1)), dma((heads, MID - 1)),
+            dma((MID - 1,)), dma((MID - 1,)),
             dma((heads, MID)), dma((heads, MID)),
             dma((heads, MID)), dma((heads, MID)),
             dma((2, 2)), dma((2, 2)),

time: 34.5 us -> 34.4 us (level)
  no operation moved by 1% of the time
where the time goes in v3:
time: 34.4 us; the launch traced here: 34.3 us
  Pallas kernels  32.4 us (94%)
  local copies, waits for them, and re-layouts  1.87 us (5%)
    pallas_call x1, Pallas kernels, per_device(): pl.pallas_call(functools.partial(kernel, sp_n, heads), out_shape=jax.Shap...  32.4 us
    unnamed x1, local copies, waits for them, and re-layouts  1.87 us

profile of v3, /device:TPU:1, one launch (start us, length us, event | category | flops | bytes accessed | tf_op | source)
XLA Modules:
  0.0 34.3 jit_solution(3925532936879382738)
XLA Ops:
  0.0 32.4 %shard_map.46 = bf16[256,1024]{1,0:T(8,128)(2,1)} custom-call(bf16[256,512]{1,0:T(8,128)(2,1)} %q_hbm.1, bf16[256,512]{1,0:T(8,128)(2,1)} %k_hbm.1, bf16[256,512]{1,0:T(8,128)(2,1)} %v_hbm.1, bf16[1024,1024]{1,0:T(8,128)(2,1)} %w_hbm.1), custom_call_target="tpu_custom_call" | custom-call | tf_op jit(solution)/shard_map/pallas_call | solution.py:356
  32.4 1.9 %copy.6 = bf16[256,1024]{1,0:T(8,128)(2,1)} copy(bf16[256,1024]{1,0:T(8,128)(2,1)} %shard_map.46) | data formatting | bytes 1048576

commit v4 on v3

--- a/solution.py
+++ b/solution.py
@@ -38,8 +38,8 @@
     return nn(raised.astype(BF16), v), top, den
 
 
-def kernel(sp_n, heads, q_hbm, k_hbm, v_hbm, w_hbm, out_ref,
-           q_in, k_in, v_in, w, pkv, kvf, near_lo, near_hi, ob, ret, att, att_other, acc_n, md_n,
+def kernel(sp_n, heads, q_hbm, k_hbm, v_hbm, out_ref,
+           q_in, k_in, v_in, pkv, kvf, near_lo, near_hi, ob, ret, att, att_other, acc_n, md_n,
            load_sem, kv_s, kv_r, q_s, q_r, up_s, up_r, dn_s, dn_r, near_s, near_r, ret_s, ret_r, tp_s, tp_r):
     rows = q_in.shape[0]
     chunk = rows // MID
@@ -51,7 +51,7 @@
 
     loads = [
         pltpu.make_async_copy(src, dst, load_sem.at[n])
-        for n, (src, dst) in enumerate(((k_hbm, k_in), (v_hbm, v_in), (q_hbm, q_in), (w_hbm, w)))
+        for n, (src, dst) in enumerate(((k_hbm, k_in), (v_hbm, v_in), (q_hbm, q_in)))
     ]
     for load in loads:
         load.start()
@@ -185,12 +185,26 @@
         for n in range(2):
             near(n, False).start()
 
+    half = rows // 2
+    own_span = half + SIDE
+    qi, ki = iota((half, own_span), 0), iota((half, own_span), 1)
+    for b in range(2):
+        at_q = slice(b * half, (b + 1) * half)
+        at_k = slice(b * (half - SIDE), b * (half - SIDE) + own_span)
+        gap = (ki + at_k.start) - (qi + at_q.start)
+        near_ok = (gap >= -SIDE) & (gap <= SIDE)
+        for h in range(heads):
+            cols = slice(h * e, (h + 1) * e)
+            o, top, den = attend(q_in[at_q, cols], k_in[at_k, cols], v_in[at_k, cols], near_ok)
+            acc_n[h, at_q, :] = o
+            md_n[h, 0, at_q, :] = jnp.broadcast_to(top, (half, e))
+            md_n[h, 1, at_q, :] = jnp.broadcast_to(den, (half, e))
+
     for h in range(heads):
         for d in range(1, MID):
             kv(h, d, receive=True).wait_recv()
             forward(h, d)
 
-    half = rows // 2
     span = half + 2 * SIDE
     qi, ki = iota((half, span), 0), iota((half, span), 1)
 
@@ -201,7 +215,8 @@
     gap = order(ki) - order(qi)
     band = (gap >= 0) & (gap <= 2 * SIDE)
     mid_ok = (band & ((ki >= SIDE) | (dn_ok == 1)), band & ((ki < span - SIDE) | (up_ok == 1)))
-    far_span = 3 * chunk
+    far_span, ns = 4 * chunk, FAR // MID
+    ones = jnp.ones((far_span, e), BF16)
     qi, ki = iota((chunk, far_span), 0), iota((chunk, far_span), 1)
     far_ok = ((ki >= qi) & (ki <= qi + 2 * SIDE) & ((ki >= chunk) | (dn_ok == 1))
               & ((ki < 2 * chunk) | (up_ok == 1)))
@@ -228,27 +243,35 @@
 
         q = kvf[h, 2, pl.ds(rows, rows), :]
         kh, vh = kvf[h, 0], kvf[h, 1]
-        mids = []
-        for b in range(2):
-            first = rows - chunk + b * half
-            mids.append(attend(q[b * half:(b + 1) * half], kh[first:first + span], vh[first:first + span], mid_ok[b]))
-        o1, t1, d1 = (jnp.concatenate([mids[0][n], mids[1][n]], axis=0) for n in range(3))
-        q4 = q.reshape(MID, FAR // MID, mm, e)
-        k4 = kh.reshape(3 * MID, FAR // MID, mm, e)
-        v4 = vh.reshape(3 * MID, FAR // MID, mm, e)
-        fars = [
-            attend(q4[:, s].reshape(chunk, e), k4[:, s].reshape(far_span, e), v4[:, s].reshape(far_span, e), far_ok)
-            for s in range(FAR // MID)
-        ]
-        o2, t2, d2 = (
-            jnp.concatenate(
-                [fars[s][n][i * mm:(i + 1) * mm] for i in range(MID) for s in range(FAR // MID)], axis=0)
-            for n in range(3))
-        top = jnp.maximum(t1, t2)
-        e1, e2 = jnp.exp2(t1 - top), jnp.exp2(t2 - top)
-        den = e1 * d1 + e2 * d2
-        o = ((e1 * o1 + e2 * o2) / den).astype(BF16)
-        log_den = jnp.broadcast_to(top + jnp.log2(den), (rows, e))
+        firsts = [rows - chunk + b * half for b in range(2)]
+        s_mid = jnp.concatenate([
+            jnp.where(mid_ok[b], nt(q[b * half:(b + 1) * half], kh[f:f + span]), -jnp.inf)
+            for b, f in enumerate(firsts)], axis=0)
+        q4 = q.reshape(MID, ns, mm, e)
+
+        def classes(x):
+            x4 = x.reshape(3 * MID, ns, mm, e)
+            return [jnp.concatenate([x4[:, n], x4[:MID, n]], axis=0).reshape(far_span, e) for n in range(ns)]
+
+        k_far, v_far = classes(kh), classes(vh)
+        far = [jnp.where(far_ok, nt(q4[:, n].reshape(chunk, e), k_far[n]), -jnp.inf) for n in range(ns)]
+        s_far = jnp.concatenate([far[n][i * mm:(i + 1) * mm] for i in range(MID) for n in range(ns)], axis=0)
+        peak = functools.reduce(
+            jnp.maximum, [x[:, i:i + e] for x in (s_mid, s_far) for i in range(0, x.shape[1], e)])
+        top = jnp.max(peak, axis=-1, keepdims=True)
+        r_mid = jnp.exp2((s_mid - top) * SCALE).astype(BF16)
+        r_far = jnp.exp2((s_far - top) * SCALE).astype(BF16)
+        total = jnp.concatenate([
+            nn(r_mid[b * half:(b + 1) * half], jnp.concatenate([vh[f:f + span], ones], axis=1))
+            for b, f in enumerate(firsts)], axis=0)
+        far = [
+            nn(jnp.concatenate([r_far[(i * ns + n) * mm:(i * ns + n + 1) * mm] for i in range(MID)], axis=0),
+               jnp.concatenate([v_far[n], ones], axis=1))
+            for n in range(ns)]
+        total += jnp.concatenate([far[n][i * mm:(i + 1) * mm] for i in range(MID) for n in range(ns)], axis=0)
+        den = total[:, e:]
+        o = (total[:, :e] / den).astype(BF16)
+        log_den = top * SCALE + jnp.log2(den)
         one = log_den.astype(BF16).astype(F32)
         two = (log_den - one).astype(BF16).astype(F32)
         three = log_den - one - two
@@ -272,21 +295,23 @@
         for n in range(2):
             near(n, False).wait_recv()
 
-    qi, ki = iota((half, span), 0), iota((half, span), 1)
-    band = (ki >= qi) & (ki <= qi + 2 * SIDE)
     lo_ok, hi_ok = has_prev.astype(jnp.int32), has_next.astype(jnp.int32)
-    allowed = (band & ((ki >= SIDE) | (lo_ok == 1)), band & ((ki < span - SIDE) | (hi_ok == 1)))
+    qi, ki = iota((SIDE, SIDE), 0), iota((SIDE, SIDE), 1)
+    corners = (
+        (near_lo, slice(0, SIDE), (ki >= qi) & (lo_ok == 1)),
+        (near_hi, slice(rows - SIDE, rows), (ki <= qi) & (hi_ok == 1)),
+    )
     for h in range(heads):
         cols = slice(h * e, (h + 1) * e)
-        ks = [jnp.concatenate([near_lo[n, :, cols], x[:, cols], near_hi[n, :, cols]], axis=0)
-              for n, x in enumerate((k_in, v_in))]
-        for b in range(2):
-            at_b = slice(b * half, (b + 1) * half)
-            o, top, den = attend(q_in[at_b, cols], ks[0][b * half:b * half + span],
-                                 ks[1][b * half:b * half + span], allowed[b])
-            acc_n[h, at_b, :] = o
-            md_n[h, 0, at_b, :] = jnp.broadcast_to(top, (half, e))
-            md_n[h, 1, at_b, :] = jnp.broadcast_to(den, (half, e))
+        for halo, at_q, ok in corners:
+            s = jnp.where(ok, nt(q_in[at_q, cols], halo[0, :, cols]) * SCALE, -jnp.inf)
+            old = md_n[h, 0, at_q, :]
+            top = jnp.maximum(old, jnp.max(s, axis=-1, keepdims=True))
+            fade = jnp.exp2(old - top)
+            raised = jnp.exp2(s - top[:, :SIDE])
+            acc_n[h, at_q, :] = fade * acc_n[h, at_q, :] + nn(raised.astype(BF16), halo[1, :, cols])
+            md_n[h, 0, at_q, :] = top
+            md_n[h, 1, at_q, :] = fade * md_n[h, 1, at_q, :] + jnp.sum(raised, axis=-1, keepdims=True)
 
     r, t = iota((rows, 2 * rows), 1), iota((rows, 2 * rows), 0)
     low = r % (2 * chunk) < chunk
@@ -310,12 +335,10 @@
         share(h).start()
 
     width = heads * e
-    loads[3].wait()
-    own = nn(att[...], w[pl.ds(pl.multiple_of(c * width, width), width), :])
+    out_ref[:, pl.ds(pl.multiple_of(c * width, width), width)] = att[...]
     for h in range(heads):
         share(h).wait_recv()
-    other = nn(att_other[...], w[pl.ds(pl.multiple_of((1 - c) * width, width), width), :])
-    out_ref[...] = (own + other).astype(BF16)
+        out_ref[:, pl.ds(pl.multiple_of((1 - c) * width + h * e, e), e)] = att_other[:, h * e:(h + 1) * e]
 
     for h in range(heads):
         for d in range(1, MID):
@@ -353,16 +376,15 @@
     assert MID * rows == SIDE * FAR and rows // MID == SIDE and sp_n % MID == 0
     dma = pltpu.SemaphoreType.DMA
     e, chunk = HEAD_DIM, rows // MID
-    return pl.pallas_call(
+    attended = pl.pallas_call(
         functools.partial(kernel, sp_n, heads),
-        out_shape=jax.ShapeDtypeStruct((rows, w.shape[1]), BF16),
-        in_specs=[pl.BlockSpec(memory_space=pl.ANY)] * 4,
+        out_shape=jax.ShapeDtypeStruct((rows, w.shape[0]), BF16),
+        in_specs=[pl.BlockSpec(memory_space=pl.ANY)] * 3,
         out_specs=pl.BlockSpec(memory_space=pltpu.VMEM),
         scratch_shapes=[
             pltpu.VMEM((rows, columns), BF16),
             pltpu.VMEM((rows, columns), BF16),
             pltpu.VMEM((rows, columns), BF16),
-            pltpu.VMEM(w.shape, BF16),
             pltpu.VMEM((heads, 3, rows, e), BF16),
             pltpu.VMEM((heads, 3, 3 * rows, e), BF16),
             pltpu.VMEM((2, SIDE, columns), BF16),
@@ -373,7 +395,7 @@
             pltpu.VMEM((rows, columns), BF16),
             pltpu.VMEM((heads, rows, e), F32),
             pltpu.VMEM((heads, 2, rows, e), F32),
-            dma((4,)),
+            dma((3,)),
             dma((heads, MID - 1)), dma((heads, MID - 1)),
             dma((MID - 1,)), dma((MID - 1,)),
             dma((heads, MID)), dma((heads, MID)),
@@ -383,7 +405,8 @@
             dma((heads,)), dma((heads,)),
         ],
         compiler_params=pltpu.CompilerParams(collective_id=0, has_side_effects=True),
-    )(q, k, v, w)
+    )(q, k, v)
+    return nn(attended, w).astype(BF16)
 
 
 def solution(mesh):

time: 34.4 us -> 30.8 us (0.90)
  Pallas kernels: 32.4 us -> 28 us
  matrix products: 0 us -> 2.55 us
  local copies, waits for them, and re-layouts: 1.87 us -> 0.01 us
    pallas_call x1, Pallas kernels: 32.4 us -> 28 us  [per_device(): pl.pallas_call(functools.partial(kernel, sp_n, heads), out_shape=jax.Shap...]
    dot_general x0 -> x1, matrix products: none -> 2.55 us  [nn(): lax.dot_general(a, b, (((1,), (0,)), ((), ())), preferred_element_type=F32)]
    unnamed x1 -> x2, local copies, waits for them, and re-layouts: 1.87 us -> 0.01 us
where the time goes in v4:
time: 30.8 us; the launch traced here: 30.6 us
  Pallas kernels  28 us (91%)
  matrix products  2.55 us (8%)
    pallas_call x1, Pallas kernels, per_device(): pl.pallas_call(functools.partial(kernel, sp_n, heads), out_shape=jax.Shap...  28 us
    dot_general x1, matrix products, nn(): lax.dot_general(a, b, (((1,), (0,)), ((), ())), preferred_element_type=F32)  2.55 us

profile of v4, /device:TPU:1, one launch (start us, length us, event | category | flops | bytes accessed | tf_op | source)
XLA Modules:
  0.0 30.6 jit_solution(1172000000721712953)
XLA Ops:
  0.0 0.0 copy-start
  0.0 28.0 %shard_map.46 = bf16[256,1024]{1,0:T(8,128)(2,1)} custom-call(bf16[256,512]{1,0:T(8,128)(2,1)} %q_hbm.1, bf16[256,512]{1,0:T(8,128)(2,1)} %k_hbm.1, bf16[256,512]{1,0:T(8,128)(2,1)} %v_hbm.1), custom_call_target="tpu_custom_call" | custom-call | tf_op jit(solution)/shard_map/pallas_call | solution.py:379
  28.0 0.0 copy-done
  28.0 2.5 %convolution_convert_fusion = bf16[256,1024]{1,0:T(8,128)(2,1)} fusion(bf16[256,1024]{1,0:T(8,128)(2,1)} %shard_map.46, bf16[1024,1024]{1,0:T(8,128)(2,1)S(1)} %copy-done), kind=kOutput, calls=%fused_computation | convolution fusion | flops 537133056 | bytes 3145728 | tf_op jit(solution)/shard_map/dot_general | solution.py:26
Async XLA Ops:
  0.0 28.0 %copy-start = (bf16[1024,1024]{1,0:T(8,128)(2,1)S(1)}, bf16[1024,1024]{1,0:T(8,128)(2,1)}, u32[]{:S(2)}) copy-start(bf16[1024,1024]{1,0:T(8,128)(2,1)} %param.7) | copy-start | bytes 6291460

commit v5 on v4

--- a/solution.py
+++ b/solution.py
@@ -40,7 +40,7 @@
 
 def kernel(sp_n, heads, q_hbm, k_hbm, v_hbm, out_ref,
            q_in, k_in, v_in, pkv, kvf, near_lo, near_hi, ob, ret, att, att_other, acc_n, md_n,
-           load_sem, kv_s, kv_r, q_s, q_r, up_s, up_r, dn_s, dn_r, near_s, near_r, ret_s, ret_r, tp_s, tp_r):
+           relay, load_sem, hop_s, hop_r, kv_s, kv_r, q_s, q_r, up_s, up_r, dn_s, dn_r, near_s, near_r, ret_s, ret_r, tp_s, tp_r):
     rows = q_in.shape[0]
     chunk = rows // MID
     mm = rows // FAR
@@ -175,15 +175,38 @@
         return remote(src.at[pl.ds(0, SIDE), :], near_hi.at[n],
                       near_s.at[n, 1], near_r.at[n, 1], (p - 1 + sp_n) % sp_n, c)
 
+    def hop(side):
+        first = (rows - SIDE, 0)[side]
+        to = ((p + MID) % sp_n, (p - MID + sp_n) % sp_n)[side]
+        return remote(v_in.at[pl.ds(first, SIDE), :], relay.at[side], near_s.at[1, side], hop_r.at[side], to, c)
+
+    def pass_on(side):
+        dst = (near_lo, near_hi)[side]
+        return remote(relay.at[side], dst.at[1], hop_s.at[side], near_r.at[1, side], mate((1, MID - 1)[side]), c)
+
     @pl.when(has_next)
     def _():
-        for n in range(2):
-            near(n, True).start()
+        near(0, True).start()
 
     @pl.when(has_prev)
     def _():
-        for n in range(2):
-            near(n, False).start()
+        near(0, False).start()
+
+    @pl.when(has_next & (j < MID - 1))
+    def _():
+        near(1, True).start()
+
+    @pl.when(has_prev & (j > 0))
+    def _():
+        near(1, False).start()
+
+    @pl.when(has_up & (j == MID - 1))
+    def _():
+        hop(0).start()
+
+    @pl.when(has_dn & (j == 0))
+    def _():
+        hop(1).start()
 
     half = rows // 2
     own_span = half + SIDE
@@ -204,6 +227,13 @@
         for d in range(1, MID):
             kv(h, d, receive=True).wait_recv()
             forward(h, d)
+
+    relays = (has_dn & (j == MID - 1), has_up & (j == 0))
+    for side in range(2):
+        @pl.when(relays[side])
+        def _():
+            hop(side).wait_recv()
+            pass_on(side).start()
 
     span = half + 2 * SIDE
     qi, ki = iota((half, span), 0), iota((half, span), 1)
@@ -347,6 +377,10 @@
         share(h).wait_send()
     for d in range(1, MID):
         queries(d).wait_send()
+    for side in range(2):
+        @pl.when(relays[side])
+        def _():
+            pass_on(side).wait_send()
     @pl.when(has_up)
     def _():
         for h in range(heads):
@@ -395,7 +429,9 @@
             pltpu.VMEM((rows, columns), BF16),
             pltpu.VMEM((heads, rows, e), F32),
             pltpu.VMEM((heads, 2, rows, e), F32),
+            pltpu.VMEM((2, SIDE, columns), BF16),
             dma((3,)),
+            dma((2,)), dma((2,)),
             dma((heads, MID - 1)), dma((heads, MID - 1)),
             dma((MID - 1,)), dma((MID - 1,)),
             dma((heads, MID)), dma((heads, MID)),

time: 30.8 us -> 30 us (0.974)
  Pallas kernels: 28 us -> 27.2 us
    pallas_call x1, Pallas kernels: 28 us -> 27.2 us  [per_device(): pl.pallas_call(functools.partial(kernel, sp_n, heads), out_shape=jax.Shap...]
where the time goes in v5:
time: 30 us; the launch traced here: 29.8 us
  Pallas kernels  27.2 us (91%)
  matrix products  2.55 us (8%)
    pallas_call x1, Pallas kernels, per_device(): pl.pallas_call(functools.partial(kernel, sp_n, heads), out_shape=jax.Shap...  27.2 us
    dot_general x1, matrix products, nn(): lax.dot_general(a, b, (((1,), (0,)), ((), ())), preferred_element_type=F32)  2.55 us

profile of v5, /device:TPU:1, one launch (start us, length us, event | category | flops | bytes accessed | tf_op | source)
XLA Modules:
  0.0 29.8 jit_solution(2099319537296044539)
XLA Ops:
  0.0 0.0 copy-start
  0.0 27.2 %shard_map.46 = bf16[256,1024]{1,0:T(8,128)(2,1)} custom-call(bf16[256,512]{1,0:T(8,128)(2,1)} %q_hbm.1, bf16[256,512]{1,0:T(8,128)(2,1)} %k_hbm.1, bf16[256,512]{1,0:T(8,128)(2,1)} %v_hbm.1), custom_call_target="tpu_custom_call" | custom-call | tf_op jit(solution)/shard_map/pallas_call | solution.py:413
  27.2 0.0 copy-done
  27.2 2.5 %convolution_convert_fusion = bf16[256,1024]{1,0:T(8,128)(2,1)} fusion(bf16[256,1024]{1,0:T(8,128)(2,1)} %shard_map.46, bf16[1024,1024]{1,0:T(8,128)(2,1)S(1)} %copy-done), kind=kOutput, calls=%fused_computation | convolution fusion | flops 537133056 | bytes 3145728 | tf_op jit(solution)/shard_map/dot_general | solution.py:26
Async XLA Ops:
  0.0 27.2 %copy-start = (bf16[1024,1024]{1,0:T(8,128)(2,1)S(1)}, bf16[1024,1024]{1,0:T(8,128)(2,1)}, u32[]{:S(2)}) copy-start(bf16[1024,1024]{1,0:T(8,128)(2,1)} %param.7) | copy-start | bytes 6291460
